TPU v7x, 32 devices: a whole 2x2x4 slice. The times are simulated.
32 devices in a mesh: sp: 8 (over z, y), tp: 4 (over x, core).
Axes of the slice: x: 2, y: 2, z: 4, core: 2. Of those that a mesh axis runs over, the one named last changes fastest.
Arguments:
- queries: bfloat16 [4096, 1024], P('sp', 'tp'), may hold values from -6 to 6
- key_heads: bfloat16 [4096, 512], P('sp', 'tp'), may hold values from -6 to 6
- value_heads: bfloat16 [4096, 512], P('sp', 'tp'), may hold values from -70 to 70
- documents: int32 [4096], P('sp'), may hold values from 0 to 2, never falling along the last dimension, each value on 1 to 2560 neighbouring positions
- query_gain: float32 [128], replicated, may hold values from 0.1 to 8
- key_gain: float32 [128], replicated, may hold values from 0.1 to 8
- out_gain: float32 [1024], replicated, may hold values from 0.1 to 1.9
- out_proj: bfloat16 [1024, 2048], replicated, may hold values from -0.1875 to 0.1875
- residual: bfloat16 [4096, 2048], P(('sp', 'tp')), may hold values from -6 to 6
- mid_gain: float32 [2048], replicated, may hold values from 0.1 to 1.9
- mid_bias: float32 [2048], replicated, may hold values from -1.5 to 1.5
- routes: int32 [4096, 2], P(('sp', 'tp')), may hold values from 0 to 31, all different within a row; in each aligned block of 128 rows (0 to 127, 128 to 255, ...) at most 16 rows name the same one
- route_weights: float32 [4096, 2], P(('sp', 'tp')), may hold values from 0.2 to 2
- expert_gate: bfloat16 [32, 2048, 512], P(('sp', 'tp')), may hold values from -0.125 to 0.125
- expert_up: bfloat16 [32, 2048, 512], P(('sp', 'tp')), may hold values from -0.125 to 0.125
- expert_down: bfloat16 [32, 512, 2048], P(('sp', 'tp')), may hold values from -0.25 to 0.25
- final_gain: float32 [2048], replicated, may hold values from 0.1 to 1.9
- final_bias: float32 [2048], replicated, may hold values from -1.5 to 1.5
Outputs:
- layer_out: bfloat16 [4096, 2048], P(('sp', 'tp'))
Inputs may be any that keep to these rules, and one draw needn't show every extreme that they name: `documents`: never falls along the sequence; each document holds 1 to 2560 positions and one holds exactly 2560. `routes`: each row names 2 different experts; among the rows of one device (aligned blocks of 128 rows) no expert is named more than 16 times, and exactly 16 times in some block.
All inputs are finite; a program needn't handle non-finite values.
Results may differ from a plain program's by a relative error of at most 0.014.
The roundings to bfloat16 on the way count: a program that leaves them out, or rounds other values in their place, can miss the bound.
Values may be sent and summed in bfloat16 or wider, within the bound.
A program may use at most 128 MiB of HBM per device.

v0:
```python
import math
import jax
import jax.numpy as jnp
from jax import lax
from jax.sharding import PartitionSpec as P

HEAD = 128
GRID = 64
eps_norm = 1e-06
alpha_mix = 8.0**0.25
theta_base = 10000.0


def rotary_tables(row_total, offset):
    positions = offset + jnp.arange(row_total, dtype=jnp.int32)
    grid_row = (positions // GRID).astype(jnp.float32)
    grid_col = (positions % GRID).astype(jnp.float32)
    pair_count = HEAD // 4
    inv_freq = theta_base ** (-jnp.arange(pair_count, dtype=jnp.float32) / pair_count)
    angles = jnp.concatenate(
        [grid_row[:, None] * inv_freq[None, :], grid_col[:, None] * inv_freq[None, :]], axis=1
    )
    return (jnp.cos(angles), jnp.sin(angles))


def normed_rotated(heads_in, gain_vec, cosine_table, sine_table):
    values = heads_in.astype(jnp.float32)
    inv_rms = lax.rsqrt(jnp.mean(values * values, axis=-1, keepdims=True) + eps_norm)
    values = values * inv_rms * gain_vec
    half_dim = HEAD // 2
    first_half = values[..., :half_dim]
    second_half = values[..., half_dim:]
    cosine_part = cosine_table[:, None, :]
    sine_part = sine_table[:, None, :]
    turned = jnp.concatenate(
        [
            first_half * cosine_part - second_half * sine_part,
            second_half * cosine_part + first_half * sine_part,
        ],
        axis=-1,
    )
    return turned.astype(jnp.bfloat16)


def layer_norm(stream, gain_vec, bias_vec):
    center = jnp.mean(stream, axis=-1, keepdims=True)
    spread = jnp.mean(jnp.square(stream - center), axis=-1, keepdims=True)
    return (stream - center) * lax.rsqrt(spread + eps_norm) * gain_vec + bias_vec


def per_device(
    queries,
    key_heads,
    value_heads,
    documents,
    query_gain,
    key_gain,
    out_gain,
    out_proj,
    residual,
    mid_gain,
    mid_bias,
    routes,
    route_weights,
    expert_gate,
    expert_up,
    expert_down,
    final_gain,
    final_bias,
):
    tok_rows = queries.shape[0]
    query_local = queries.shape[1] // HEAD
    key_local = key_heads.shape[1] // HEAD
    grouped = query_local // key_local
    offset = lax.axis_index("sp") * tok_rows
    cosine_table, sine_table = rotary_tables(tok_rows, offset)
    query_rot = normed_rotated(
        queries.reshape(tok_rows, query_local, HEAD), query_gain, cosine_table, sine_table
    ).reshape(tok_rows, key_local, grouped, HEAD)
    key_rot = normed_rotated(
        key_heads.reshape(tok_rows, key_local, HEAD), key_gain, cosine_table, sine_table
    ).reshape(tok_rows, key_local * HEAD)
    first_doc = documents[0]
    last_doc = documents[tok_rows - 1]
    start_state = (
        jnp.full((key_local, grouped, tok_rows), -1e30, jnp.float32),
        jnp.zeros((key_local, grouped, tok_rows), jnp.float32),
        jnp.zeros((key_local, grouped, tok_rows, HEAD), jnp.float32),
    )
    key_part = lax.all_gather(key_rot, "sp", axis=0, tiled=True)
    value_part = lax.all_gather(value_heads, "sp", axis=0, tiled=True)
    doc_part = lax.all_gather(documents, "sp", axis=0, tiled=True)
    piece_rows = key_part.shape[0]
    block_rows = math.gcd(piece_rows, 512)
    block_count = piece_rows // block_rows
    blocks = (
        key_part.reshape(block_count, block_rows, key_local, HEAD),
        value_part.reshape(block_count, block_rows, key_local, HEAD),
        doc_part.reshape(block_count, block_rows),
    )

    def advance(running, block_set):
        key_block, value_block, doc_block = block_set
        running_max, running_total, running_sum = running
        scores = jnp.einsum(
            "qkgd,tkd->kgqt", query_rot, key_block, preferred_element_type=jnp.float32
        ) * HEAD ** (-0.5)
        allowed = (documents[:, None] == doc_block[None, :])[None, None]
        scores = jnp.where(allowed, scores, -1e30)
        new_max = jnp.maximum(running_max, jnp.max(scores, axis=-1))
        weights = jnp.where(allowed, jnp.exp(scores - new_max[..., None]), 0.0)
        rescale = jnp.exp(running_max - new_max)
        new_total = running_total * rescale + jnp.sum(weights, axis=-1)
        new_sum = running_sum * rescale[..., None] + jnp.einsum(
            "kgqt,tkd->kgqd",
            weights.astype(jnp.bfloat16),
            value_block,
            preferred_element_type=jnp.float32,
        )
        return ((new_max, new_total, new_sum), None)

    def process(running):
        result, unused = lax.scan(advance, running, blocks)
        return result

    touches = (doc_part[0] <= last_doc) & (doc_part[piece_rows - 1] >= first_doc)
    final_max, final_total, final_sum = lax.cond(
        touches, process, lambda running: running, start_state
    )
    attention = jnp.transpose(final_sum / final_total[..., None], (2, 0, 1, 3))
    attention = attention.reshape(tok_rows, query_local * HEAD).astype(jnp.bfloat16)
    whole_rows = lax.all_to_all(attention, "tp", split_axis=0, concat_axis=1, tiled=True)
    whole_float = whole_rows.astype(jnp.float32)
    mean_square = jnp.mean(whole_float * whole_float, axis=1)
    scaled = (whole_float * out_gain).astype(jnp.bfloat16)
    projected = jnp.dot(scaled, out_proj, preferred_element_type=jnp.float32)
    projected = projected * lax.rsqrt(mean_square + eps_norm)[:, None]
    middle = layer_norm(
        alpha_mix * residual.astype(jnp.float32) + projected, mid_gain, mid_bias
    ).astype(jnp.bfloat16)
    out_rows = middle.shape[0]
    model_width = middle.shape[1]
    top_count = routes.shape[1]
    local_experts = expert_gate.shape[0]
    sp_size = lax.axis_size("sp")
    tp_size = lax.axis_size("tp")
    expert_total = local_experts * sp_size * tp_size
    capacity = 2 * out_rows * top_count // expert_total
    flat_routes = routes.reshape(-1)
    one_hot = (flat_routes[:, None] == jnp.arange(expert_total, dtype=jnp.int32)[None, :]).astype(
        jnp.int32
    )
    rank_in = jnp.sum((jnp.cumsum(one_hot, axis=0) - one_hot) * one_hot, axis=1)
    target = flat_routes * capacity + rank_in
    outbound = (
        jnp.zeros((expert_total * capacity, model_width), jnp.bfloat16)
        .at[target]
        .set(jnp.repeat(middle, top_count, axis=0))
    )
    arrived = lax.all_to_all(
        outbound.reshape(expert_total, capacity, model_width),
        ("sp", "tp"),
        split_axis=0,
        concat_axis=0,
        tiled=True,
    )
    item_count = arrived.shape[-2]
    grouped_rows = arrived.reshape(-1, local_experts, item_count, model_width)
    gate_part = jnp.einsum(
        "sekd,edf->sekf", grouped_rows, expert_gate, preferred_element_type=jnp.float32
    )
    up_part = jnp.einsum(
        "sekd,edf->sekf", grouped_rows, expert_up, preferred_element_type=jnp.float32
    )
    hidden = (jax.nn.silu(gate_part) * up_part).astype(jnp.bfloat16)
    served = jnp.einsum("sekf,efd->sekd", hidden, expert_down, preferred_element_type=jnp.float32)
    returned = lax.all_to_all(
        served.astype(jnp.bfloat16).reshape(arrived.shape),
        ("sp", "tp"),
        split_axis=0,
        concat_axis=0,
        tiled=True,
    )
    picked = returned.reshape(expert_total * capacity, model_width)[target]
    picked = picked.astype(jnp.float32).reshape(out_rows, top_count, model_width)
    routed = jnp.sum(picked * route_weights[:, :, None], axis=1)
    return layer_norm(
        alpha_mix * middle.astype(jnp.float32) + routed, final_gain, final_bias
    ).astype(jnp.bfloat16)


def solution(mesh):
    return jax.shard_map(
        per_device,
        mesh=mesh,
        in_specs=(
            P("sp", "tp"),
            P("sp", "tp"),
            P("sp", "tp"),
            P("sp"),
            P(),
            P(),
            P(),
            P(),
            P(("sp", "tp"), None),
            P(),
            P(),
            P(("sp", "tp"), None),
            P(("sp", "tp"), None),
            P(("sp", "tp"), None, None),
            P(("sp", "tp"), None, None),
            P(("sp", "tp"), None, None),
            P(),
            P(),
        ),
        out_specs=P(("sp", "tp"), None),
        check_vma=False,
    )
```

profile of v0, /device:TPU:0, one launch (start us, length us, event | category | flops | bytes accessed | tf_op | source)
XLA Modules:
  0.0 323.6 jit_solution(3362261494470061725)
XLA Ops:
  11.2 27.9 %all-gather = s32[8,1,512]{2,1,0:T(1,128)S(1)} all-gather(s32[1,1,512]{2,1,0:T(1,128)S(1)} %bitcast.186), channel_id=1, replica_groups=mesh['sp'=8,'tp'=4] {'sp'}, dimensions={0}, use_global_device_ids=true | all-gather | bytes 18432 | tf_op jit(solution)/shard_map/all_gather | solution.py:92
  44.9 7.3 %all-gather.4.cloned.1.call-done = bf16[4096,128]{0,1:T(8,128)(2,1)} async-done(((bf16[512,128]{0,1:T(8,128)(2,1)}), bf16[4096,128]{0,1:T(8,128)(2,1)}) %all-gather.4.cloned.1.call-update) | async-done | bytes 1048592 | tf_op jit(solution)/shard_map/all_gather | solution.py:90
  52.2 41.4 %all-gather.6.cloned.1.call-done = bf16[4096,128]{1,0:T(8,128)(2,1)} async-done(((bf16[512,128]{1,0:T(8,128)(2,1)}), bf16[4096,128]{1,0:T(8,128)(2,1)}) %all-gather.6.cloned.1.call-update) | async-done | bytes 1048592 | tf_op jit(solution)/shard_map/all_gather | solution.py:91
  93.6 69.2 %conditional.1 = (f32[1,2,512]{2,1,0:T(2,128)}, f32[1,2,512,128]{3,2,1,0:T(8,128)}) conditional(s32[]{:T(128)} %bitcast.4, () %tuple.17, (bf16[4096,128]{0,1:T(8,128)(2,1)}, bf16[4096,128]{1,0:T(8,128)(2,1)}, s32[4096]{0:T(1024)S(1)}, s32[512]{0:T(512)S(1)}, bf16[512,1,2,128]{0,3,2,1:T(8,128)(2,1)S(1)}) %tuple.62), branch_computations={%region_2.3_spmd, %region_3.8_spmd} | conditional | flops 275912704 | bytes 20030728 | solution.py:127
  96.1 66.7 %while.14 = (s32[]{:T(128)}, f32[1,2,512]{2,1,0:T(2,128)S(1)}, f32[1,2,512]{2,1,0:T(2,128)}, f32[1,2,512,128]{3,2,1,0:T(8,128)}, s32[512]{0:T(512)S(1)}, /*index...) while((s32[]{:T(128)}, f32[1,2,512]{2,1,0:T(2,128)S(1)}, ...), condition=%wide.region_7.7_spmd.clone, body=%wide.region_4.6_spmd.clone.sunk | while | flops 275912704 | bytes 17376408 | solution.py:123
  99.2 3.4 %fusion.96 = f32[1,2,512,128]{3,2,1,0:T(8,128)} fusion(f32[512,512,2]{1,0,2:T(8,128)} %get-tuple-element.223, f32[2,512]{1,0:T(2,128)S(1)} %bitcast.183, pred[512,512]{0,1:T(8,128)(4,1)S(1)} %broadcast_compare_fusion.2, f32[1,2,512,128]{3,2,1,0:T(8,128)} %get-tuple-element.239, f32[2,512]{1,0:T(2,128)S(1)} %get-tuple-element.224, pred[]{:T(512)S(6)} %compare.14, ...), kind=kOutput, calls=%fused_computation.8.clone.1 | convolution fusion | flops 137232384 | bytes 3547649 | tf_op jit(solution)/shard_map/cond/branch_1_fun/while/body/eval_jaxpr/kgqt,tkd->kgqd/dot_general | solution.py:114
  106.8 3.5 %fusion.96 = f32[1,2,512,128]{3,2,1,0:T(8,128)} fusion(f32[512,512,2]{1,0,2:T(8,128)} %get-tuple-element.223, f32[2,512]{1,0:T(2,128)S(1)} %bitcast.183, pred[512,512]{0,1:T(8,128)(4,1)S(1)} %broadcast_compare_fusion.2, f32[1,2,512,128]{3,2,1,0:T(8,128)} %get-tuple-element.239, f32[2,512]{1,0:T(2,128)S(1)} %get-tuple-element.224, pred[]{:T(512)S(6)} %compare.14, ...), kind=kOutput, calls=%fused_computation.8.clone.1 | convolution fusion | flops 137232384 | bytes 3547649 | tf_op jit(solution)/shard_map/cond/branch_1_fun/while/body/eval_jaxpr/kgqt,tkd->kgqd/dot_general | solution.py:114
  115.3 3.5 %fusion.96 = f32[1,2,512,128]{3,2,1,0:T(8,128)} fusion(f32[512,512,2]{1,0,2:T(8,128)} %get-tuple-element.223, f32[2,512]{1,0:T(2,128)S(1)} %bitcast.183, pred[512,512]{0,1:T(8,128)(4,1)S(1)} %broadcast_compare_fusion.2, f32[1,2,512,128]{3,2,1,0:T(8,128)} %get-tuple-element.239, f32[2,512]{1,0:T(2,128)S(1)} %get-tuple-element.224, pred[]{:T(512)S(6)} %compare.14, ...), kind=kOutput, calls=%fused_computation.8.clone.1 | convolution fusion | flops 137232384 | bytes 3547649 | tf_op jit(solution)/shard_map/cond/branch_1_fun/while/body/eval_jaxpr/kgqt,tkd->kgqd/dot_general | solution.py:114
  123.7 3.5 %fusion.96 = f32[1,2,512,128]{3,2,1,0:T(8,128)} fusion(f32[512,512,2]{1,0,2:T(8,128)} %get-tuple-element.223, f32[2,512]{1,0:T(2,128)S(1)} %bitcast.183, pred[512,512]{0,1:T(8,128)(4,1)S(1)} %broadcast_compare_fusion.2, f32[1,2,512,128]{3,2,1,0:T(8,128)} %get-tuple-element.239, f32[2,512]{1,0:T(2,128)S(1)} %get-tuple-element.224, pred[]{:T(512)S(6)} %compare.14, ...), kind=kOutput, calls=%fused_computation.8.clone.1 | convolution fusion | flops 137232384 | bytes 3547649 | tf_op jit(solution)/shard_map/cond/branch_1_fun/while/body/eval_jaxpr/kgqt,tkd->kgqd/dot_general | solution.py:114
  132.1 3.5 %fusion.96 = f32[1,2,512,128]{3,2,1,0:T(8,128)} fusion(f32[512,512,2]{1,0,2:T(8,128)} %get-tuple-element.223, f32[2,512]{1,0:T(2,128)S(1)} %bitcast.183, pred[512,512]{0,1:T(8,128)(4,1)S(1)} %broadcast_compare_fusion.2, f32[1,2,512,128]{3,2,1,0:T(8,128)} %get-tuple-element.239, f32[2,512]{1,0:T(2,128)S(1)} %get-tuple-element.224, pred[]{:T(512)S(6)} %compare.14, ...), kind=kOutput, calls=%fused_computation.8.clone.1 | convolution fusion | flops 137232384 | bytes 3547649 | tf_op jit(solution)/shard_map/cond/branch_1_fun/while/body/eval_jaxpr/kgqt,tkd->kgqd/dot_general | solution.py:114
  140.6 3.5 %fusion.96 = f32[1,2,512,128]{3,2,1,0:T(8,128)} fusion(f32[512,512,2]{1,0,2:T(8,128)} %get-tuple-element.223, f32[2,512]{1,0:T(2,128)S(1)} %bitcast.183, pred[512,512]{0,1:T(8,128)(4,1)S(1)} %broadcast_compare_fusion.2, f32[1,2,512,128]{3,2,1,0:T(8,128)} %get-tuple-element.239, f32[2,512]{1,0:T(2,128)S(1)} %get-tuple-element.224, pred[]{:T(512)S(6)} %compare.14, ...), kind=kOutput, calls=%fused_computation.8.clone.1 | convolution fusion | flops 137232384 | bytes 3547649 | tf_op jit(solution)/shard_map/cond/branch_1_fun/while/body/eval_jaxpr/kgqt,tkd->kgqd/dot_general | solution.py:114
  149.0 3.5 %fusion.96 = f32[1,2,512,128]{3,2,1,0:T(8,128)} fusion(f32[512,512,2]{1,0,2:T(8,128)} %get-tuple-element.223, f32[2,512]{1,0:T(2,128)S(1)} %bitcast.183, pred[512,512]{0,1:T(8,128)(4,1)S(1)} %broadcast_compare_fusion.2, f32[1,2,512,128]{3,2,1,0:T(8,128)} %get-tuple-element.239, f32[2,512]{1,0:T(2,128)S(1)} %get-tuple-element.224, pred[]{:T(512)S(6)} %compare.14, ...), kind=kOutput, calls=%fused_computation.8.clone.1 | convolution fusion | flops 137232384 | bytes 3547649 | tf_op jit(solution)/shard_map/cond/branch_1_fun/while/body/eval_jaxpr/kgqt,tkd->kgqd/dot_general | solution.py:114
  157.4 3.5 %fusion.96 = f32[1,2,512,128]{3,2,1,0:T(8,128)} fusion(f32[512,512,2]{1,0,2:T(8,128)} %get-tuple-element.223, f32[2,512]{1,0:T(2,128)S(1)} %bitcast.183, pred[512,512]{0,1:T(8,128)(4,1)S(1)} %broadcast_compare_fusion.2, f32[1,2,512,128]{3,2,1,0:T(8,128)} %get-tuple-element.239, f32[2,512]{1,0:T(2,128)S(1)} %get-tuple-element.224, pred[]{:T(512)S(6)} %compare.14, ...), kind=kOutput, calls=%fused_computation.8.clone.1 | convolution fusion | flops 137232384 | bytes 3547649 | tf_op jit(solution)/shard_map/cond/branch_1_fun/while/body/eval_jaxpr/kgqt,tkd->kgqd/dot_general | solution.py:114
  165.2 3.4 %all-to-all-start = ((bf16[4,128,256]{2,1,0:T(8,128)(2,1)}), bf16[4,128,256]{2,1,0:T(8,128)(2,1)S(1)}, u32[]{:S(2)}, u32[]{:S(2)}) async-start(bf16[4,128,256]{2,1,0:T(8,128)(2,1)} %convert_element_type.116), calls=%async_computation | async-start | bytes 524288 | tf_op jit(solution)/shard_map/all_to_all | solution.py:132
  168.7 6.0 %all-to-all-done = bf16[4,128,256]{2,1,0:T(8,128)(2,1)S(1)} async-done(((bf16[4,128,256]{2,1,0:T(8,128)(2,1)}), bf16[4,128,256]{2,1,0:T(8,128)(2,1)S(1)}, u32[]{:S(2)}, u32[]{:S(2)}) %all-to-all-start) | async-done | bytes 262176 | tf_op jit(solution)/shard_map/all_to_all | solution.py:132
  175.3 3.1 fusion.80
  182.8 4.4 %scatter_custom_fusion = bf16[512,2048]{1,0:T(8,128)(2,1)} fusion(s32[256]{0:T(256)S(1)} %bitcast.190, bf16[256,2048]{1,0:T(8,128)(2,1)} %reshape.481, bf16[]{:T(256)} %constant.103.clone.1), kind=kCustom, calls=%fused_computation.51 | custom fusion | bytes 2097664 | tf_op jit(solution)/shard_map/scatter | solution.py:158
  187.3 51.5 %all_to_all.20 = bf16[32,16,2048]{2,1,0:T(8,128)(2,1)S(1)} all-to-all(bf16[32,16,2048]{2,1,0:T(8,128)(2,1)} %bitcast.181), channel_id=1, replica_groups=mesh['sp'=8,'tp'=4] {'sp','tp'}, dimensions={0} | all-to-all | bytes 4194304 | tf_op jit(solution)/shard_map/all_to_all | solution.py:160
  242.3 6.3 %convolution_convert_fusion = bf16[32,16,2048]{2,1,0:T(8,128)(2,1)} fusion(bf16[1,512,2048]{2,1,0:T(8,128)(2,1)S(1)} %copy-done, bf16[32,16,2048]{2,1,0:T(8,128)(2,1)} %copy-done.2, bf16[1,2048,512]{2,1,0:T(8,128)(2,1)} %param.36, f32[32,1,16,512]{3,2,0,1:T(8,128)} %fusion.29), kind=kOutput, calls=%fused_computation.35 | convolution fusion | flops 2150105088 | bytes 9437184 | tf_op jit(solution)/shard_map/sekf,efd->sekd/dot_general | solution.py:176
  248.6 3.7 %all-to-all-start.2 = ((bf16[32,16,2048]{2,1,0:T(8,128)(2,1)}), bf16[32,16,2048]{2,1,0:T(8,128)(2,1)}, u32[]{:S(2)}, u32[]{:S(2)}) async-start(bf16[32,16,2048]{2,1,0:T(8,128)(2,1)} %convolution_convert_fusion), calls=%async_computation.2 | async-start | bytes 4194304 | tf_op jit(solution)/shard_map/all_to_all | solution.py:177
  252.4 48.6 %all-to-all-done.2 = bf16[32,16,2048]{2,1,0:T(8,128)(2,1)} async-done(((bf16[32,16,2048]{2,1,0:T(8,128)(2,1)}), bf16[32,16,2048]{2,1,0:T(8,128)(2,1)}, u32[]{:S(2)}, u32[]{:S(2)}) %all-to-all-start.2) | async-done | bytes 2097184 | tf_op jit(solution)/shard_map/all_to_all | solution.py:177
  301.0 5.2 %gather_fusion = bf16[256,2048]{1,0:T(8,128)(2,1)} fusion(bf16[512,2048]{1,0:T(8,128)(2,1)} %bitcast.37, s32[1024]{0:T(1024)S(1)} %pad_clamp_fusion), kind=kCustom, calls=%fused_computation | custom fusion | bytes 2098176 | tf_op jit(solution)/shard_map/gather | solution.py:184
  306.2 3.4 %reshape.468 = f32[128,2,2048]{2,1,0:T(2,128)} reshape(bf16[256,2048]{1,0:T(8,128)(2,1)} %gather_fusion) | data formatting | bytes 3145728 | tf_op jit(solution)/shard_map/convert_element_type | solution.py:185
  309.6 4.8 %multiply_reduce_fusion = f32[128,2048]{1,0:T(8,128)S(1)} fusion(f32[128,2,2048]{2,1,0:T(2,128)} %reshape.468, f32[128,2]{1,0:T(8,128)S(1)} %copy.56), kind=kLoop, calls=%fused_computation.43 | loop fusion | flops 786432 | bytes 3146752 | tf_op jit(solution)/shard_map/reduce_sum | solution.py:186
  (161 shorter events, 62.0 us)
Async XLA Ops:
  6.5 235.8 %copy-start = (bf16[1,512,2048]{2,1,0:T(8,128)(2,1)S(1)}, bf16[1,512,2048]{2,1,0:T(8,128)(2,1)}, u32[]{:S(2)}) copy-start(bf16[1,512,2048]{2,1,0:T(8,128)(2,1)} %param.37) | copy-start | bytes 6291460
  6.5 4.1 %copy-start.10 = (s32[128,2]{0,1:T(2,128)S(1)}, s32[128,2]{0,1:T(2,128)}, u32[]{:S(2)}) copy-start(s32[128,2]{0,1:T(2,128)} %param.33) | copy-start | bytes 3076
  6.5 4.5 %copy-start.3 = (bf16[512,256]{1,0:T(8,128)(2,1)S(1)}, bf16[512,256]{1,0:T(8,128)(2,1)}, u32[]{:S(2)}) copy-start(bf16[512,256]{1,0:T(8,128)(2,1)} %param.22) | copy-start | bytes 786436
  6.5 4.7 %copy-start.6 = (s32[512]{0:T(512)S(1)}, s32[512]{0:T(512)}, u32[]{:S(2)}) copy-start(s32[512]{0:T(512)} %param.25) | copy-start | bytes 6148
  6.5 38.1 %copy-start.12 = (f32[128]{0:T(128)S(1)}, f32[128]{0:T(128)}, u32[]{:S(2)}) copy-start(f32[128]{0:T(128)} %param.26) | copy-start | bytes 1540
  6.5 45.6 %all-gather.4.cloned.1.call-start = ((), (), s32[]{:S(2)}) async-start(), calls=%async_computation.3 | async-start | bytes 1179648 | tf_op jit(solution)/shard_map/all_gather | solution.py:90
  9.9 83.7 %all-gather.6.cloned.1.call-start = ((), (), s32[]{:S(2)}) async-start(), calls=%async_computation.4 | async-start | bytes 1179648 | tf_op jit(solution)/shard_map/all_gather | solution.py:91
  99.2 3.4 %copy-start.1 = (f32[512,512,2]{1,0,2:T(8,128)S(1)}, f32[512,512,2]{1,0,2:T(8,128)}, u32[]{:S(2)}) copy-start(f32[512,512,2]{1,0,2:T(8,128)} %get-tuple-element.223) | copy-start | bytes 6291460 | tf_op jit(solution)/shard_map/cond/branch_1_fun/while
  106.8 3.5 %copy-start.1 = (f32[512,512,2]{1,0,2:T(8,128)S(1)}, f32[512,512,2]{1,0,2:T(8,128)}, u32[]{:S(2)}) copy-start(f32[512,512,2]{1,0,2:T(8,128)} %get-tuple-element.223) | copy-start | bytes 6291460 | tf_op jit(solution)/shard_map/cond/branch_1_fun/while
  115.3 3.5 %copy-start.1 = (f32[512,512,2]{1,0,2:T(8,128)S(1)}, f32[512,512,2]{1,0,2:T(8,128)}, u32[]{:S(2)}) copy-start(f32[512,512,2]{1,0,2:T(8,128)} %get-tuple-element.223) | copy-start | bytes 6291460 | tf_op jit(solution)/shard_map/cond/branch_1_fun/while
  123.7 3.5 %copy-start.1 = (f32[512,512,2]{1,0,2:T(8,128)S(1)}, f32[512,512,2]{1,0,2:T(8,128)}, u32[]{:S(2)}) copy-start(f32[512,512,2]{1,0,2:T(8,128)} %get-tuple-element.223) | copy-start | bytes 6291460 | tf_op jit(solution)/shard_map/cond/branch_1_fun/while
  132.1 3.5 %copy-start.1 = (f32[512,512,2]{1,0,2:T(8,128)S(1)}, f32[512,512,2]{1,0,2:T(8,128)}, u32[]{:S(2)}) copy-start(f32[512,512,2]{1,0,2:T(8,128)} %get-tuple-element.223) | copy-start | bytes 6291460 | tf_op jit(solution)/shard_map/cond/branch_1_fun/while
  140.6 3.5 %copy-start.1 = (f32[512,512,2]{1,0,2:T(8,128)S(1)}, f32[512,512,2]{1,0,2:T(8,128)}, u32[]{:S(2)}) copy-start(f32[512,512,2]{1,0,2:T(8,128)} %get-tuple-element.223) | copy-start | bytes 6291460 | tf_op jit(solution)/shard_map/cond/branch_1_fun/while
  149.0 3.5 %copy-start.1 = (f32[512,512,2]{1,0,2:T(8,128)S(1)}, f32[512,512,2]{1,0,2:T(8,128)}, u32[]{:S(2)}) copy-start(f32[512,512,2]{1,0,2:T(8,128)} %get-tuple-element.223) | copy-start | bytes 6291460 | tf_op jit(solution)/shard_map/cond/branch_1_fun/while
  157.4 3.5 %copy-start.1 = (f32[512,512,2]{1,0,2:T(8,128)S(1)}, f32[512,512,2]{1,0,2:T(8,128)}, u32[]{:S(2)}) copy-start(f32[512,512,2]{1,0,2:T(8,128)} %get-tuple-element.223) | copy-start | bytes 6291460 | tf_op jit(solution)/shard_map/cond/branch_1_fun/while
  162.8 12.2 %copy-start.9 = (f32[1024]{0:T(1024)S(1)}, f32[1024]{0:T(1024)}, u32[]{:S(2)}) copy-start(f32[1024]{0:T(1024)} %param.28) | copy-start | bytes 12292
  165.2 9.4 %all-to-all-start = ((bf16[4,128,256]{2,1,0:T(8,128)(2,1)}), bf16[4,128,256]{2,1,0:T(8,128)(2,1)S(1)}, u32[]{:S(2)}, u32[]{:S(2)}) async-start(bf16[4,128,256]{2,1,0:T(8,128)(2,1)} %convert_element_type.116), calls=%async_computation | async-start | bytes 524288 | tf_op jit(solution)/shard_map/all_to_all | solution.py:132
  175.2 3.4 %copy-start.4 = (f32[2048]{0:T(1024)S(1)}, f32[2048]{0:T(1024)}, u32[]{:S(2)}) copy-start(f32[2048]{0:T(1024)} %param.32) | copy-start | bytes 24580
  175.2 3.4 %copy-start.5 = (f32[2048]{0:T(1024)S(1)}, f32[2048]{0:T(1024)}, u32[]{:S(2)}) copy-start(f32[2048]{0:T(1024)} %param.31) | copy-start | bytes 24580
  187.3 52.8 %copy-start.13 = (bf16[1,2048,512]{2,1,0:T(8,128)(2,1)S(1)}, bf16[1,2048,512]{2,1,0:T(8,128)(2,1)}, u32[]{:S(2)}) copy-start(bf16[1,2048,512]{2,1,0:T(8,128)(2,1)} %param.35) | copy-start | bytes 6291460
  238.8 1.3 copy-start.2
  248.6 3.7 %copy-start.11 = (f32[128,2]{0,1:T(2,128)S(1)}, f32[128,2]{0,1:T(2,128)}, u32[]{:S(2)}) copy-start(f32[128,2]{0,1:T(2,128)} %param.34) | copy-start | bytes 3076
  248.6 52.4 %all-to-all-start.2 = ((bf16[32,16,2048]{2,1,0:T(8,128)(2,1)}), bf16[32,16,2048]{2,1,0:T(8,128)(2,1)}, u32[]{:S(2)}, u32[]{:S(2)}) async-start(bf16[32,16,2048]{2,1,0:T(8,128)(2,1)} %convolution_convert_fusion), calls=%async_computation.2 | async-start | bytes 4194304 | tf_op jit(solution)/shard_map/all_to_all | solution.py:177
  314.4 0.9 copy-start.7
  (1 other events, 0.9 us)
Sparse Core Ops, SparseCore 0:
  10.0 42.1 all-gather.3
  54.3 39.2 all-gather.5
where the time goes:
time: 325 us; the launch traced here: 324 us
  waiting for transfers between devices  104 us (32%)
  blocking collectives  79.5 us (24%)
  matrix products  62.1 us (19%)
  other arithmetic  28.8 us (9%)
  local copies, waits for them, and re-layouts  25.6 us (8%)
  between operations  16.3 us (5%)
  starting transfers between devices  7.21 us (2%)
    all_to_all x1, blocking collectives, per_device(): lax.all_to_all(outbound.reshape(expert_total, capacity, model_width), ('s...  51.5 us
    all_to_all x1, waiting for transfers between devices, per_device(): lax.all_to_all(served.astype(jnp.bfloat16).reshape(arrived.shape), ('sp',...  48.6 us
    all_gather x1, waiting for transfers between devices, per_device(): value_part = lax.all_gather(value_heads, 'sp', axis=0, tiled=True)  41.4 us
    dot_general x8, matrix products, advance(): jnp.einsum('kgqt,tkd->kgqd', weights.astype(jnp.bfloat16), value_block, p...  28 us
    all_gather x1, blocking collectives, per_device(): doc_part = lax.all_gather(documents, 'sp', axis=0, tiled=True)  27.9 us
    dot_general x8, matrix products, advance(): jnp.einsum('qkgd,tkd->kgqt', query_rot, key_block, preferred_element_type...  22.4 us
    add x8, other arithmetic, advance(): new_total = running_total * rescale + jnp.sum(weights, axis=-1)  9.54 us
    all_gather x1, waiting for transfers between devices, per_device(): key_part = lax.all_gather(key_rot, 'sp', axis=0, tiled=True)  7.31 us
  transfers between devices with their start and end apart: 4, of which 4 were waited for; matrix products, arithmetic and copies ran while one was open for 1% of the time, Pallas kernels for 0%

commit v1 on v0

--- a/solution.py
+++ b/solution.py
@@ -88,7 +88,9 @@
         jnp.zeros((key_local, grouped, tok_rows, HEAD), jnp.float32),
     )
     key_part = lax.all_gather(key_rot, "sp", axis=0, tiled=True)
-    value_part = lax.all_gather(value_heads, "sp", axis=0, tiled=True)
+    value_part = jnp.concatenate(
+        lax.all_to_all(jnp.stack([value_heads] * lax.axis_size("sp")), "sp", 0, 0), axis=0
+    )
     doc_part = lax.all_gather(documents, "sp", axis=0, tiled=True)
     piece_rows = key_part.shape[0]
     block_rows = math.gcd(piece_rows, 512)

time: 325 us -> 304 us (0.935)
  waiting for transfers between devices: 104 us -> 54.6 us
  blocking collectives: 79.5 us -> 99.8 us
  starting transfers between devices: 7.21 us -> 14.6 us
    all_gather x1 -> x0, waiting for transfers between devices: 41.4 us -> none  [per_device(): value_part = lax.all_gather(value_heads, 'sp', axis=0, tiled=True)]
    all_gather x1, blocking collectives: 27.9 us -> 48.3 us  [per_device(): doc_part = lax.all_gather(documents, 'sp', axis=0, tiled=True)]
    all_to_all x0 -> x1, starting transfers between devices: none -> 7.44 us  [per_device(): lax.all_to_all(jnp.stack([value_heads] * lax.axis_size('sp')), 'sp', 0, 0)]
    all_gather x1, waiting for transfers between devices: 7.31 us -> 0.02 us  [per_device(): key_part = lax.all_gather(key_rot, 'sp', axis=0, tiled=True)]
  transfers between devices with their start and end apart: 4 -> 4, of which waited for: 4 -> 2; matrix products, arithmetic and copies ran while one was open for 1% -> 2% of each run, Pallas kernels for 0% -> 0%
where the time goes in v1:
time: 304 us; the launch traced here: 303 us
  blocking collectives  99.8 us (33%)
  matrix products  62.1 us (20%)
  waiting for transfers between devices  54.6 us (18%)
  other arithmetic  28.8 us (9%)
  local copies, waits for them, and re-layouts  26.7 us (9%)
  between operations  16.3 us (5%)
  starting transfers between devices  14.6 us (5%)
    all_to_all x1, blocking collectives, per_device(): lax.all_to_all(outbound.reshape(expert_total, capacity, model_width), ('s...  51.5 us
    all_to_all x1, waiting for transfers between devices, per_device(): lax.all_to_all(served.astype(jnp.bfloat16).reshape(arrived.shape), ('sp',...  48.6 us
    all_gather x1, blocking collectives, per_device(): doc_part = lax.all_gather(documents, 'sp', axis=0, tiled=True)  48.3 us
    dot_general x8, matrix products, advance(): jnp.einsum('kgqt,tkd->kgqd', weights.astype(jnp.bfloat16), value_block, p...  28 us
    dot_general x8, matrix products, advance(): jnp.einsum('qkgd,tkd->kgqt', query_rot, key_block, preferred_element_type...  22.4 us
    add x8, other arithmetic, advance(): new_total = running_total * rescale + jnp.sum(weights, axis=-1)  9.54 us
    all_to_all x1, starting transfers between devices, per_device(): lax.all_to_all(jnp.stack([value_heads] * lax.axis_size('sp')), 'sp', 0, 0)  7.44 us
    dot_general x1, matrix products, per_device(): jnp.einsum('sekf,efd->sekd', hidden, expert_down, preferred_element_type=...  6.27 us
  transfers between devices with their start and end apart: 4, of which 2 were waited for; matrix products, arithmetic and copies ran while one was open for 2% of the time, Pallas kernels for 0%

profile of v1, /device:TPU:0, one launch (start us, length us, event | category | flops | bytes accessed | tf_op | source)
XLA Modules:
  0.0 303.1 jit_solution(1333772610361120397)
XLA Ops:
  11.0 7.4 %all-to-all-start = ((bf16[8,512,128]{2,1,0:T(8,128)(2,1)}), bf16[8,512,128]{2,1,0:T(8,128)(2,1)}, u32[]{:S(2)}, u32[]{:S(2)}) async-start(bf16[8,512,128]{2,1,0:T(8,128)(2,1)} %stack.2), calls=%async_computation | async-start | bytes 2097152 | tf_op jit(solution)/shard_map/all_to_all | solution.py:92
  19.0 48.3 %all-gather = s32[8,1,512]{2,1,0:T(1,128)S(1)} all-gather(s32[1,1,512]{2,1,0:T(1,128)S(1)} %bitcast.186), channel_id=1, replica_groups=mesh['sp'=8,'tp'=4] {'sp'}, dimensions={0}, use_global_device_ids=true | all-gather | bytes 18432 | tf_op jit(solution)/shard_map/all_gather | solution.py:94
  73.1 69.2 %conditional.1 = (f32[1,2,512]{2,1,0:T(2,128)}, f32[1,2,512,128]{3,2,1,0:T(8,128)}) conditional(s32[]{:T(128)} %bitcast.4, () %tuple.17, (bf16[4096,128]{0,1:T(8,128)(2,1)}, bf16[8,512,128]{2,1,0:T(8,128)(2,1)}, s32[4096]{0:T(1024)S(1)}, s32[512]{0:T(512)S(1)}, bf16[512,1,2,128]{0,3,2,1:T(8,128)(2,1)S(1)}) %tuple.60), branch_computations={%region_2.3_spmd, %region_3.8_spmd} | conditional | flops 275912704 | bytes 20030728 | solution.py:129
  75.6 66.7 %while.14 = (s32[]{:T(128)}, f32[1,2,512]{2,1,0:T(2,128)S(1)}, f32[1,2,512]{2,1,0:T(2,128)}, f32[1,2,512,128]{3,2,1,0:T(8,128)}, s32[512]{0:T(512)S(1)}, /*index...) while((s32[]{:T(128)}, f32[1,2,512]{2,1,0:T(2,128)S(1)}, ...), condition=%wide.region_7.7_spmd.clone, body=%wide.region_4.6_spmd.clone.sunk | while | flops 275912704 | bytes 17376408 | solution.py:125
  78.7 3.4 %fusion.96 = f32[1,2,512,128]{3,2,1,0:T(8,128)} fusion(f32[512,512,2]{1,0,2:T(8,128)} %get-tuple-element.223, f32[2,512]{1,0:T(2,128)S(1)} %bitcast.183, pred[512,512]{0,1:T(8,128)(4,1)S(1)} %broadcast_compare_fusion.2, f32[1,2,512,128]{3,2,1,0:T(8,128)} %get-tuple-element.239, f32[2,512]{1,0:T(2,128)S(1)} %get-tuple-element.224, pred[]{:T(512)S(6)} %compare.14, ...), kind=kOutput, calls=%fused_computation.8.clone.1 | convolution fusion | flops 137232384 | bytes 3547649 | tf_op jit(solution)/shard_map/cond/branch_1_fun/while/body/eval_jaxpr/kgqt,tkd->kgqd/dot_general | solution.py:116
  86.4 3.5 %fusion.96 = f32[1,2,512,128]{3,2,1,0:T(8,128)} fusion(f32[512,512,2]{1,0,2:T(8,128)} %get-tuple-element.223, f32[2,512]{1,0:T(2,128)S(1)} %bitcast.183, pred[512,512]{0,1:T(8,128)(4,1)S(1)} %broadcast_compare_fusion.2, f32[1,2,512,128]{3,2,1,0:T(8,128)} %get-tuple-element.239, f32[2,512]{1,0:T(2,128)S(1)} %get-tuple-element.224, pred[]{:T(512)S(6)} %compare.14, ...), kind=kOutput, calls=%fused_computation.8.clone.1 | convolution fusion | flops 137232384 | bytes 3547649 | tf_op jit(solution)/shard_map/cond/branch_1_fun/while/body/eval_jaxpr/kgqt,tkd->kgqd/dot_general | solution.py:116
  92.0 2.8 fusion.93
  94.8 3.5 %fusion.96 = f32[1,2,512,128]{3,2,1,0:T(8,128)} fusion(f32[512,512,2]{1,0,2:T(8,128)} %get-tuple-element.223, f32[2,512]{1,0:T(2,128)S(1)} %bitcast.183, pred[512,512]{0,1:T(8,128)(4,1)S(1)} %broadcast_compare_fusion.2, f32[1,2,512,128]{3,2,1,0:T(8,128)} %get-tuple-element.239, f32[2,512]{1,0:T(2,128)S(1)} %get-tuple-element.224, pred[]{:T(512)S(6)} %compare.14, ...), kind=kOutput, calls=%fused_computation.8.clone.1 | convolution fusion | flops 137232384 | bytes 3547649 | tf_op jit(solution)/shard_map/cond/branch_1_fun/while/body/eval_jaxpr/kgqt,tkd->kgqd/dot_general | solution.py:116
  103.2 3.5 %fusion.96 = f32[1,2,512,128]{3,2,1,0:T(8,128)} fusion(f32[512,512,2]{1,0,2:T(8,128)} %get-tuple-element.223, f32[2,512]{1,0:T(2,128)S(1)} %bitcast.183, pred[512,512]{0,1:T(8,128)(4,1)S(1)} %broadcast_compare_fusion.2, f32[1,2,512,128]{3,2,1,0:T(8,128)} %get-tuple-element.239, f32[2,512]{1,0:T(2,128)S(1)} %get-tuple-element.224, pred[]{:T(512)S(6)} %compare.14, ...), kind=kOutput, calls=%fused_computation.8.clone.1 | convolution fusion | flops 137232384 | bytes 3547649 | tf_op jit(solution)/shard_map/cond/branch_1_fun/while/body/eval_jaxpr/kgqt,tkd->kgqd/dot_general | solution.py:116
  111.7 3.5 %fusion.96 = f32[1,2,512,128]{3,2,1,0:T(8,128)} fusion(f32[512,512,2]{1,0,2:T(8,128)} %get-tuple-element.223, f32[2,512]{1,0:T(2,128)S(1)} %bitcast.183, pred[512,512]{0,1:T(8,128)(4,1)S(1)} %broadcast_compare_fusion.2, f32[1,2,512,128]{3,2,1,0:T(8,128)} %get-tuple-element.239, f32[2,512]{1,0:T(2,128)S(1)} %get-tuple-element.224, pred[]{:T(512)S(6)} %compare.14, ...), kind=kOutput, calls=%fused_computation.8.clone.1 | convolution fusion | flops 137232384 | bytes 3547649 | tf_op jit(solution)/shard_map/cond/branch_1_fun/while/body/eval_jaxpr/kgqt,tkd->kgqd/dot_general | solution.py:116
  120.1 3.5 %fusion.96 = f32[1,2,512,128]{3,2,1,0:T(8,128)} fusion(f32[512,512,2]{1,0,2:T(8,128)} %get-tuple-element.223, f32[2,512]{1,0:T(2,128)S(1)} %bitcast.183, pred[512,512]{0,1:T(8,128)(4,1)S(1)} %broadcast_compare_fusion.2, f32[1,2,512,128]{3,2,1,0:T(8,128)} %get-tuple-element.239, f32[2,512]{1,0:T(2,128)S(1)} %get-tuple-element.224, pred[]{:T(512)S(6)} %compare.14, ...), kind=kOutput, calls=%fused_computation.8.clone.1 | convolution fusion | flops 137232384 | bytes 3547649 | tf_op jit(solution)/shard_map/cond/branch_1_fun/while/body/eval_jaxpr/kgqt,tkd->kgqd/dot_general | solution.py:116
  128.5 3.5 %fusion.96 = f32[1,2,512,128]{3,2,1,0:T(8,128)} fusion(f32[512,512,2]{1,0,2:T(8,128)} %get-tuple-element.223, f32[2,512]{1,0:T(2,128)S(1)} %bitcast.183, pred[512,512]{0,1:T(8,128)(4,1)S(1)} %broadcast_compare_fusion.2, f32[1,2,512,128]{3,2,1,0:T(8,128)} %get-tuple-element.239, f32[2,512]{1,0:T(2,128)S(1)} %get-tuple-element.224, pred[]{:T(512)S(6)} %compare.14, ...), kind=kOutput, calls=%fused_computation.8.clone.1 | convolution fusion | flops 137232384 | bytes 3547649 | tf_op jit(solution)/shard_map/cond/branch_1_fun/while/body/eval_jaxpr/kgqt,tkd->kgqd/dot_general | solution.py:116
  137.0 3.5 %fusion.96 = f32[1,2,512,128]{3,2,1,0:T(8,128)} fusion(f32[512,512,2]{1,0,2:T(8,128)} %get-tuple-element.223, f32[2,512]{1,0:T(2,128)S(1)} %bitcast.183, pred[512,512]{0,1:T(8,128)(4,1)S(1)} %broadcast_compare_fusion.2, f32[1,2,512,128]{3,2,1,0:T(8,128)} %get-tuple-element.239, f32[2,512]{1,0:T(2,128)S(1)} %get-tuple-element.224, pred[]{:T(512)S(6)} %compare.14, ...), kind=kOutput, calls=%fused_computation.8.clone.1 | convolution fusion | flops 137232384 | bytes 3547649 | tf_op jit(solution)/shard_map/cond/branch_1_fun/while/body/eval_jaxpr/kgqt,tkd->kgqd/dot_general | solution.py:116
  144.8 3.4 %all-to-all-start.1 = ((bf16[4,128,256]{2,1,0:T(8,128)(2,1)}), bf16[4,128,256]{2,1,0:T(8,128)(2,1)S(1)}, u32[]{:S(2)}, u32[]{:S(2)}) async-start(bf16[4,128,256]{2,1,0:T(8,128)(2,1)} %convert_element_type.116), calls=%async_computation.1 | async-start | bytes 524288 | tf_op jit(solution)/shard_map/all_to_all | solution.py:134
  148.2 6.0 %all-to-all-done.1 = bf16[4,128,256]{2,1,0:T(8,128)(2,1)S(1)} async-done(((bf16[4,128,256]{2,1,0:T(8,128)(2,1)}), bf16[4,128,256]{2,1,0:T(8,128)(2,1)S(1)}, u32[]{:S(2)}, u32[]{:S(2)}) %all-to-all-start.1) | async-done | bytes 262176 | tf_op jit(solution)/shard_map/all_to_all | solution.py:134
  154.8 3.1 %fusion.80 = (f32[128]{0:T(128)S(1)}, f32[128,2048]{1,0:T(8,128)S(1)}) fusion(f32[128]{0:T(128)S(1)} %add_rsqrt_fusion.4, bf16[128,1024]{0,1:T(8,128)(2,1)S(1)} %fusion.51, bf16[1024,2048]{1,0:T(8,128)(2,1)} %param.29, bf16[128,2048]{1,0:T(8,128)(2,1)} %param.30), kind=kOutput, calls=%fused_computation.129 | convolution fusion | flops 538181504 | bytes 6030336 | tf_op jit(solution)/shard_map/dot_general | solution.py:138
  162.3 4.4 %scatter_custom_fusion = bf16[512,2048]{1,0:T(8,128)(2,1)} fusion(s32[256]{0:T(256)S(1)} %bitcast.190, bf16[256,2048]{1,0:T(8,128)(2,1)} %reshape.479, bf16[]{:T(256)} %constant.103.clone.1), kind=kCustom, calls=%fused_computation.51 | custom fusion | bytes 2097664 | tf_op jit(solution)/shard_map/scatter | solution.py:160
  166.8 51.5 %all_to_all.25 = bf16[32,16,2048]{2,1,0:T(8,128)(2,1)S(1)} all-to-all(bf16[32,16,2048]{2,1,0:T(8,128)(2,1)} %bitcast.181), channel_id=1, replica_groups=mesh['sp'=8,'tp'=4] {'sp','tp'}, dimensions={0} | all-to-all | bytes 4194304 | tf_op jit(solution)/shard_map/all_to_all | solution.py:162
  221.8 6.3 %convolution_convert_fusion = bf16[32,16,2048]{2,1,0:T(8,128)(2,1)} fusion(bf16[1,512,2048]{2,1,0:T(8,128)(2,1)S(1)} %copy-done, bf16[32,16,2048]{2,1,0:T(8,128)(2,1)} %copy-done.2, bf16[1,2048,512]{2,1,0:T(8,128)(2,1)} %param.36, f32[32,1,16,512]{3,2,0,1:T(8,128)} %fusion.29), kind=kOutput, calls=%fused_computation.35 | convolution fusion | flops 2150105088 | bytes 9437184 | tf_op jit(solution)/shard_map/sekf,efd->sekd/dot_general | solution.py:178
  228.1 3.7 %all-to-all-start.3 = ((bf16[32,16,2048]{2,1,0:T(8,128)(2,1)}), bf16[32,16,2048]{2,1,0:T(8,128)(2,1)}, u32[]{:S(2)}, u32[]{:S(2)}) async-start(bf16[32,16,2048]{2,1,0:T(8,128)(2,1)} %convolution_convert_fusion), calls=%async_computation.3 | async-start | bytes 4194304 | tf_op jit(solution)/shard_map/all_to_all | solution.py:179
  231.9 48.6 %all-to-all-done.3 = bf16[32,16,2048]{2,1,0:T(8,128)(2,1)} async-done(((bf16[32,16,2048]{2,1,0:T(8,128)(2,1)}), bf16[32,16,2048]{2,1,0:T(8,128)(2,1)}, u32[]{:S(2)}, u32[]{:S(2)}) %all-to-all-start.3) | async-done | bytes 2097184 | tf_op jit(solution)/shard_map/all_to_all | solution.py:179
  280.5 5.2 %gather_fusion = bf16[256,2048]{1,0:T(8,128)(2,1)} fusion(bf16[512,2048]{1,0:T(8,128)(2,1)} %bitcast.37, s32[1024]{0:T(1024)S(1)} %pad_clamp_fusion), kind=kCustom, calls=%fused_computation | custom fusion | bytes 2098176 | tf_op jit(solution)/shard_map/gather | solution.py:186
  285.7 3.4 %reshape.466 = f32[128,2,2048]{2,1,0:T(2,128)} reshape(bf16[256,2048]{1,0:T(8,128)(2,1)} %gather_fusion) | data formatting | bytes 3145728 | tf_op jit(solution)/shard_map/convert_element_type | solution.py:187
  289.1 4.8 %multiply_reduce_fusion = f32[128,2048]{1,0:T(8,128)S(1)} fusion(f32[128,2,2048]{2,1,0:T(2,128)} %reshape.466, f32[128,2]{1,0:T(8,128)S(1)} %copy.56), kind=kLoop, calls=%fused_computation.43 | loop fusion | flops 786432 | bytes 3146752 | tf_op jit(solution)/shard_map/reduce_sum | solution.py:188
  (163 shorter events, 59.6 us)
Async XLA Ops:
  6.5 215.3 %copy-start = (bf16[1,512,2048]{2,1,0:T(8,128)(2,1)S(1)}, bf16[1,512,2048]{2,1,0:T(8,128)(2,1)}, u32[]{:S(2)}) copy-start(bf16[1,512,2048]{2,1,0:T(8,128)(2,1)} %param.37) | copy-start | bytes 6291460
  6.5 3.3 %copy-start.6 = (bf16[512,128]{1,0:T(8,128)(2,1)S(1)}, bf16[512,128]{1,0:T(8,128)(2,1)}, u32[]{:S(2)}) copy-start(bf16[512,128]{1,0:T(8,128)(2,1)} %param.24) | copy-start | bytes 393220
  6.5 66.6 %all-gather.3.cloned.1.call-start = ((), (), s32[]{:S(2)}) async-start(), calls=%async_computation.4 | async-start | bytes 1179648 | tf_op jit(solution)/shard_map/all_gather | solution.py:90
  8.7 9.8 %copy-start.11 = (s32[128,2]{0,1:T(2,128)S(1)}, s32[128,2]{0,1:T(2,128)}, u32[]{:S(2)}) copy-start(s32[128,2]{0,1:T(2,128)} %param.33) | copy-start | bytes 3076
  8.7 10.2 %copy-start.3 = (bf16[512,256]{1,0:T(8,128)(2,1)S(1)}, bf16[512,256]{1,0:T(8,128)(2,1)}, u32[]{:S(2)}) copy-start(bf16[512,256]{1,0:T(8,128)(2,1)} %param.22) | copy-start | bytes 786436
  9.8 9.2 %copy-start.7 = (s32[512]{0:T(512)S(1)}, s32[512]{0:T(512)}, u32[]{:S(2)}) copy-start(s32[512]{0:T(512)} %param.25) | copy-start | bytes 6148
  11.0 61.8 %copy-start.13 = (f32[128]{0:T(128)S(1)}, f32[128]{0:T(128)}, u32[]{:S(2)}) copy-start(f32[128]{0:T(128)} %param.26) | copy-start | bytes 1540
  11.0 62.1 %all-to-all-start = ((bf16[8,512,128]{2,1,0:T(8,128)(2,1)}), bf16[8,512,128]{2,1,0:T(8,128)(2,1)}, u32[]{:S(2)}, u32[]{:S(2)}) async-start(bf16[8,512,128]{2,1,0:T(8,128)(2,1)} %stack.2), calls=%async_computation | async-start | bytes 2097152 | tf_op jit(solution)/shard_map/all_to_all | solution.py:92
  78.7 3.4 %copy-start.1 = (f32[512,512,2]{1,0,2:T(8,128)S(1)}, f32[512,512,2]{1,0,2:T(8,128)}, u32[]{:S(2)}) copy-start(f32[512,512,2]{1,0,2:T(8,128)} %get-tuple-element.223) | copy-start | bytes 6291460 | tf_op jit(solution)/shard_map/cond/branch_1_fun/while
  86.3 3.5 %copy-start.1 = (f32[512,512,2]{1,0,2:T(8,128)S(1)}, f32[512,512,2]{1,0,2:T(8,128)}, u32[]{:S(2)}) copy-start(f32[512,512,2]{1,0,2:T(8,128)} %get-tuple-element.223) | copy-start | bytes 6291460 | tf_op jit(solution)/shard_map/cond/branch_1_fun/while
  94.8 3.5 %copy-start.1 = (f32[512,512,2]{1,0,2:T(8,128)S(1)}, f32[512,512,2]{1,0,2:T(8,128)}, u32[]{:S(2)}) copy-start(f32[512,512,2]{1,0,2:T(8,128)} %get-tuple-element.223) | copy-start | bytes 6291460 | tf_op jit(solution)/shard_map/cond/branch_1_fun/while
  103.2 3.5 %copy-start.1 = (f32[512,512,2]{1,0,2:T(8,128)S(1)}, f32[512,512,2]{1,0,2:T(8,128)}, u32[]{:S(2)}) copy-start(f32[512,512,2]{1,0,2:T(8,128)} %get-tuple-element.223) | copy-start | bytes 6291460 | tf_op jit(solution)/shard_map/cond/branch_1_fun/while
  111.6 3.5 %copy-start.1 = (f32[512,512,2]{1,0,2:T(8,128)S(1)}, f32[512,512,2]{1,0,2:T(8,128)}, u32[]{:S(2)}) copy-start(f32[512,512,2]{1,0,2:T(8,128)} %get-tuple-element.223) | copy-start | bytes 6291460 | tf_op jit(solution)/shard_map/cond/branch_1_fun/while
  120.1 3.5 %copy-start.1 = (f32[512,512,2]{1,0,2:T(8,128)S(1)}, f32[512,512,2]{1,0,2:T(8,128)}, u32[]{:S(2)}) copy-start(f32[512,512,2]{1,0,2:T(8,128)} %get-tuple-element.223) | copy-start | bytes 6291460 | tf_op jit(solution)/shard_map/cond/branch_1_fun/while
  128.5 3.5 %copy-start.1 = (f32[512,512,2]{1,0,2:T(8,128)S(1)}, f32[512,512,2]{1,0,2:T(8,128)}, u32[]{:S(2)}) copy-start(f32[512,512,2]{1,0,2:T(8,128)} %get-tuple-element.223) | copy-start | bytes 6291460 | tf_op jit(solution)/shard_map/cond/branch_1_fun/while
  136.9 3.5 %copy-start.1 = (f32[512,512,2]{1,0,2:T(8,128)S(1)}, f32[512,512,2]{1,0,2:T(8,128)}, u32[]{:S(2)}) copy-start(f32[512,512,2]{1,0,2:T(8,128)} %get-tuple-element.223) | copy-start | bytes 6291460 | tf_op jit(solution)/shard_map/cond/branch_1_fun/while
  142.3 12.2 %copy-start.10 = (f32[1024]{0:T(1024)S(1)}, f32[1024]{0:T(1024)}, u32[]{:S(2)}) copy-start(f32[1024]{0:T(1024)} %param.28) | copy-start | bytes 12292
  144.8 9.4 %all-to-all-start.1 = ((bf16[4,128,256]{2,1,0:T(8,128)(2,1)}), bf16[4,128,256]{2,1,0:T(8,128)(2,1)S(1)}, u32[]{:S(2)}, u32[]{:S(2)}) async-start(bf16[4,128,256]{2,1,0:T(8,128)(2,1)} %convert_element_type.116), calls=%async_computation.1 | async-start | bytes 524288 | tf_op jit(solution)/shard_map/all_to_all | solution.py:134
  154.7 3.4 %copy-start.4 = (f32[2048]{0:T(1024)S(1)}, f32[2048]{0:T(1024)}, u32[]{:S(2)}) copy-start(f32[2048]{0:T(1024)} %param.32) | copy-start | bytes 24580
  154.8 3.4 %copy-start.5 = (f32[2048]{0:T(1024)S(1)}, f32[2048]{0:T(1024)}, u32[]{:S(2)}) copy-start(f32[2048]{0:T(1024)} %param.31) | copy-start | bytes 24580
  166.8 52.8 %copy-start.14 = (bf16[1,2048,512]{2,1,0:T(8,128)(2,1)S(1)}, bf16[1,2048,512]{2,1,0:T(8,128)(2,1)}, u32[]{:S(2)}) copy-start(bf16[1,2048,512]{2,1,0:T(8,128)(2,1)} %param.35) | copy-start | bytes 6291460
  218.3 1.3 copy-start.2
  228.1 3.7 %copy-start.12 = (f32[128,2]{0,1:T(2,128)S(1)}, f32[128,2]{0,1:T(2,128)}, u32[]{:S(2)}) copy-start(f32[128,2]{0,1:T(2,128)} %param.34) | copy-start | bytes 3076
  228.1 52.4 %all-to-all-start.3 = ((bf16[32,16,2048]{2,1,0:T(8,128)(2,1)}), bf16[32,16,2048]{2,1,0:T(8,128)(2,1)}, u32[]{:S(2)}, u32[]{:S(2)}) async-start(bf16[32,16,2048]{2,1,0:T(8,128)(2,1)} %convolution_convert_fusion), calls=%async_computation.3 | async-start | bytes 4194304 | tf_op jit(solution)/shard_map/all_to_all | solution.py:179
  (2 other events, 1.9 us)
Sparse Core Ops, SparseCore 0:
  10.0 52.4 all-gather.2
